TPU v7x, 32 devices: a whole 2x2x4 slice. The times are simulated.
32 devices in a mesh: ep: 8 (over z, core), tp: 4 (over y, x).
Axes of the slice: x: 2, y: 2, z: 4, core: 2. Of those that a mesh axis runs over, the one named last changes fastest.
Arguments:
- branch_in: bfloat16 [8192, 512], P(('ep', 'tp')), may hold values from -6 to 6
- pool_weight: bfloat16 [4, 128, 128], replicated, may hold values from -0.5 to 0.5
- group_gain: float32 [512], replicated, may hold values from 0.1 to 1.9
- out_weight: bfloat16 [512, 2048], P(None, 'tp'), may hold values from -0.25 to 0.25
- out_gain: float32 [2048], replicated, may hold values from 0.1 to 1.9
- ffn_input: bfloat16 [1024, 2048], P('ep'), may hold values from -6 to 6
- ffn_gain: float32 [2048], replicated, may hold values from 0.1 to 1.9
- routes: int32 [1024, 4], P('ep'), may hold values from 0 to 7, all different within a row; in each aligned block of 128 rows (0 to 127, 128 to 255, ...) at most 128 rows name the same one
- route_weight: float32 [1024, 4], P('ep'), may hold values from 0.2 to 2
- gate_weight: bfloat16 [8, 2048, 4096], P('ep', None, 'tp'), may hold values from -0.375 to 0.375
- up_weight: bfloat16 [8, 2048, 4096], P('ep', None, 'tp'), may hold values from -0.375 to 0.375
- down_weight: bfloat16 [8, 4096, 2048], P('ep', 'tp'), may hold values from -0.0078125 to 0.0078125
Outputs:
- mixer_out: bfloat16 [8192, 2048], P(('ep', 'tp'))
- expert_out: bfloat16 [1024, 2048], P('ep', 'tp')
Inputs may be any that keep to these rules, and one draw needn't show every extreme that they name: `routes`: each row names 4 different experts. Among the 128 rows of one index of ep no expert is named by more than 128 rows, and in some such block one expert is named by exactly 128.
All inputs are finite; a program needn't handle non-finite values.
Results may differ from a plain program's by a relative error of at most 0.017.
Values may be sent and summed in bfloat16 or wider, within the bound.
A program may use at most 64 MiB of HBM per device.

v0:
```python
import jax
import jax.numpy as jnp
from jax import lax
from jax.sharding import PartitionSpec as P

pool_windows = (2, 4, 8, 16)
rim_rows = 15
norm_eps = 1e-06
clamp_limit = 7.0
sigmoid_slope = 1.702


def shifted_2(block, axis, distance):
    devices = range(lax.axis_size(axis))
    route = [(i - distance, i) for i in devices if i - distance in devices]
    return lax.ppermute(block, axis, route)


def rms_scale(values, gain):
    return values * lax.rsqrt(jnp.mean(values * values, axis=-1, keepdims=True) + norm_eps) * gain


def slot_tables(route_block, expert_count, capacity):
    row_count, top_count = route_block.shape
    flat_experts = route_block.reshape(-1)
    one_hot = (flat_experts[:, None] == jnp.arange(expert_count, dtype=jnp.int32)[None, :]).astype(
        jnp.int32
    )
    earlier = jnp.cumsum(one_hot, axis=0) - one_hot
    slot_index = jnp.sum(earlier * one_hot, axis=1)
    flat_slots = slot_index * expert_count + flat_experts
    owner_rows = jnp.full((capacity * expert_count,), row_count, jnp.int32)
    owner_rows = owner_rows.at[flat_slots].set(
        jnp.arange(row_count * top_count, dtype=jnp.int32) // top_count
    )
    return (flat_slots, owner_rows)


def pool_branch(branch_in, pool_weight, group_gain, out_weight, out_gain):
    row_count, width = branch_in.shape
    group_chans = width // len(pool_windows)
    rim = shifted_2(branch_in[row_count - rim_rows :], ("ep", "tp"), 1)
    widened = jnp.concatenate([rim, branch_in], axis=0).astype(jnp.float32)
    first_row = (lax.axis_index("ep") * lax.axis_size("tp") + lax.axis_index("tp")) * row_count
    positions = first_row + jnp.arange(row_count, dtype=jnp.int32)
    window = jnp.repeat(jnp.array(pool_windows, jnp.int32), group_chans)
    summed = jnp.zeros((row_count, width), jnp.float32)
    for offset_back in range(rim_rows + 1):
        shifted = widened[rim_rows - offset_back : rim_rows - offset_back + row_count]
        summed = summed + jnp.where(window[None, :] > offset_back, shifted, jnp.float32(0.0))
    counts = jnp.minimum(window[None, :], positions[:, None] + 1).astype(jnp.float32)
    pooled = (summed / counts - widened[rim_rows:]).astype(jnp.bfloat16)
    mixed_parts = []
    for group_index in range(len(pool_windows)):
        lower = group_index * group_chans
        mixed_parts.append(
            jnp.dot(
                pooled[:, lower : lower + group_chans],
                pool_weight[group_index],
                preferred_element_type=jnp.float32,
            )
        )
    group_mix = jnp.concatenate(mixed_parts, axis=1)
    mixed_rows = rms_scale(group_mix, group_gain).astype(jnp.bfloat16)
    projected = jnp.dot(
        mixed_rows,
        lax.all_gather(out_weight, "tp", axis=1, tiled=True),
        preferred_element_type=jnp.float32,
    )
    return rms_scale(projected, out_gain).astype(jnp.bfloat16)


def expert_hidden(slot_rows, gate_local, up_local):
    gate_pre = jnp.einsum("sed,df->sef", slot_rows, gate_local, preferred_element_type=jnp.float32)
    up_pre = jnp.einsum("sed,df->sef", slot_rows, up_local, preferred_element_type=jnp.float32)
    gate_pre = jnp.minimum(gate_pre, clamp_limit)
    up_pre = jnp.clip(up_pre, -clamp_limit, clamp_limit)
    return ((up_pre + 1.0) * gate_pre * jax.nn.sigmoid(sigmoid_slope * gate_pre)).astype(
        jnp.bfloat16
    )


def send_home(hidden, down_local):
    partial_sum = jnp.einsum("sef,fd->sed", hidden, down_local, preferred_element_type=jnp.float32)
    partial_sum = partial_sum.astype(jnp.bfloat16).astype(jnp.float32)
    summed = lax.psum_scatter(
        partial_sum.astype(jnp.bfloat16), "tp", scatter_dimension=2, tiled=True
    )
    return lax.all_to_all(summed, "ep", split_axis=1, concat_axis=1, tiled=True)


def per_device(
    branch_in,
    pool_weight,
    group_gain,
    out_weight,
    out_gain,
    ffn_input,
    ffn_gain,
    routes,
    route_weight,
    gate_weight,
    up_weight,
    down_weight,
):
    mixer_out = pool_branch(branch_in, pool_weight, group_gain, out_weight, out_gain)
    normed_rows = rms_scale(ffn_input.astype(jnp.float32), ffn_gain).astype(jnp.bfloat16)
    row_count, model_width = normed_rows.shape
    top_count = routes.shape[1]
    expert_count = lax.axis_size("ep")
    capacity = 2 * row_count * top_count // expert_count
    flat_slots, owner_rows = slot_tables(routes, expert_count, capacity)
    padded = jnp.concatenate([normed_rows, jnp.zeros((1, model_width), jnp.bfloat16)], axis=0)
    slot_rows = padded[owner_rows].reshape(capacity, expert_count, model_width)
    gate_local = gate_weight[0]
    up_local = up_weight[0]
    down_local = down_weight[0]
    share = capacity // lax.axis_size("tp")
    my_share = lax.dynamic_slice_in_dim(slot_rows, lax.axis_index("tp") * share, share, 0)
    arrived = lax.all_to_all(my_share, "ep", split_axis=1, concat_axis=1, tiled=True)
    hidden = expert_hidden(lax.all_gather(arrived, "tp", axis=0, tiled=True), gate_local, up_local)
    returned = send_home(hidden, down_local)
    column_count = returned.shape[2]
    picked = returned.reshape(capacity * expert_count, column_count)[flat_slots]
    picked = picked.reshape(row_count, top_count, column_count).astype(jnp.float32)
    expert_out = jnp.sum(picked * route_weight[:, :, None], axis=1).astype(jnp.bfloat16)
    return (mixer_out, expert_out)


def solution(mesh):
    in_specs = (
        P(("ep", "tp"), None),
        P(),
        P(),
        P(None, "tp"),
        P(),
        P("ep", None),
        P(),
        P("ep", None),
        P("ep", None),
        P("ep", None, "tp"),
        P("ep", None, "tp"),
        P("ep", "tp", None),
    )
    out_specs = (P(("ep", "tp"), None), P("ep", "tp"))
    return jax.shard_map(
        per_device, mesh=mesh, in_specs=in_specs, out_specs=out_specs, check_vma=False
    )
```

profile of v0, /device:TPU:0, one launch (start us, length us, event | category | flops | bytes accessed | tf_op | source)
XLA Modules:
  0.0 230.9 jit_solution(12385050998380482686)
XLA Ops:
  7.2 0.0 all-gather.5.cloned.1.call-start
  7.2 0.8 copy.16
  8.0 0.1 eq.29
  8.1 0.1 eq.25
  8.2 0.1 reshape.209
  8.4 1.1 reduce-window.6
  9.5 0.2 slice_reduce_fusion
  9.8 0.1 fusion.52
  9.9 2.4 %scatter_custom_fusion = s32[1024]{0:T(1024)S(1)} fusion(s32[512]{0:T(512)S(1)} %bitcast.66, s32[512]{0:T(512)S(1)} %add_select_fusion, s32[]{:T(128)} %constant.34.clone.1), kind=kCustom, calls=%fused_computation.109 | custom fusion | bytes 4100 | tf_op jit(solution)/shard_map/scatter | solution.py:33
  12.3 1.2 fusion.11
  13.6 1.2 fusion.13
  14.9 6.0 %gather_fusion = bf16[1024,2048]{1,0:T(8,128)(2,1)} fusion(bf16[129,2048]{1,0:T(8,128)(2,1)S(1)} %concatenate.11, s32[1024]{0:T(1024)S(1)} %fusion.54), kind=kCustom, calls=%fused_computation | custom fusion | bytes 8392704 | tf_op jit(solution)/shard_map/gather | solution.py:114
  20.9 1.3 constant_dynamic-slice_fusion
  22.2 0.6 copy.22
  22.8 32.8 %all_to_all.10 = bf16[32,8,2048]{2,0,1:T(8,128)(2,1)} all-to-all(bf16[32,8,2048]{2,0,1:T(8,128)(2,1)S(1)} %copy.22), channel_id=1, replica_groups=mesh['ep'=8,'tp'=4] {'ep'}, dimensions={1} | all-to-all | bytes 2097152 | tf_op jit(solution)/shard_map/all_to_all | solution.py:120
  55.6 0.0 all-gather.5.cloned.1.call-update
  55.6 0.0 reduce-scatter.2.cloned.1.call-start
  55.7 51.6 %all-gather.5.cloned.1.call-done = bf16[128,8,2048]{2,0,1:T(8,128)(2,1)} async-done(((bf16[32,8,2048]{2,0,1:T(8,128)(2,1)}), bf16[128,8,2048]{2,0,1:T(8,128)(2,1)}) %all-gather.5.cloned.1.call-update) | async-done | bytes 4194320 | tf_op jit(solution)/shard_map/all_gather | solution.py:121
  107.3 7.6 %fusion.2 = f32[128,8,1024]{2,0,1:T(8,128)S(1)} fusion(bf16[128,8,2048]{2,0,1:T(8,128)(2,1)} %all-gather.5.cloned.1.call-done, bf16[1,2048,1024]{2,1,0:T(8,128)(2,1)} %param.22), kind=kOutput, calls=%fused_computation.5 | convolution fusion | flops 4294967296 | bytes 12582912 | tf_op jit(solution)/shard_map/sed,df->sef/dot_general | solution.py:74
  115.0 0.0 copy-start.7
  115.0 5.7 %multiply_convert_fusion = bf16[128,8,1024]{2,0,1:T(8,128)(2,1)S(1)} fusion(f32[128,8,1024]{2,0,1:T(8,128)S(1)} %fusion.2, bf16[128,8,2048]{2,0,1:T(8,128)(2,1)S(1)} %copy-done.8, bf16[1,2048,1024]{2,1,0:T(8,128)(2,1)S(1)} %copy-done.6), kind=kOutput, calls=%fused_computation.9 | convolution fusion | flops 4305453056 | bytes 14680064 | tf_op jit(solution)/shard_map/sed,df->sef/dot_general | solution.py:75
  120.6 6.1 %fusion.6 = bf16[128,8,2048]{2,0,1:T(8,128)(2,1)} fusion(bf16[128,8,1024]{2,0,1:T(8,128)(2,1)S(1)} %multiply_convert_fusion, bf16[1,1024,2048]{2,1,0:T(8,128)(2,1)S(1)} %copy-done.7), kind=kOutput, calls=%fused_computation.10 | convolution fusion | flops 4297064448 | bytes 10485760 | tf_op jit(solution)/shard_map/sef,fd->sed/dot_general | solution.py:84
  126.7 0.0 reduce-scatter.2.cloned.1.call-update
  126.7 0.0 all-gather.3.cloned.1.call-start
  126.8 0.7 all-gather.3.cloned.1.call-update
  127.5 0.2 copy-done
  127.7 3.4 %collective-permute-start = (bf16[15,512]{1,0:T(8,128)(2,1)S(1)}, bf16[15,512]{1,0:T(8,128)(2,1)S(1)}, u32[]{:S(2)}, u32[]{:S(2)}) collective-permute-start(bf16[15,512]{1,0:T(8,128)(2,1)S(1)} %slice.82), channel_id=1, source_target_pairs={{0,1},{1,2},{2,3},{3,4},{4,5},{5,6},{6,7},{7,8},{8,9},{9,10},{10,1... | collective-permute-start | bytes 46088 | tf_op jit(solution)/shard_map/ppermute | solution.py:16
  131.1 0.1 broadcast_bitcast_fusion
  131.2 0.1 bitcast_compare_fusion.15
  131.3 0.1 copy.21
  131.4 1.1 collective-permute-done
  132.5 0.1 maximum_convert_fusion
  132.6 0.0 copy-start.1
  132.6 1.1 fusion.31
  133.8 0.2 fusion.35
  134.0 45.5 %reduce-scatter.2.cloned.1.call-done = bf16[128,8,512]{2,0,1:T(8,128)(2,1)} async-done(((bf16[128,8,2048]{2,0,1:T(8,128)(2,1)}), bf16[128,8,512]{2,0,1:T(8,128)(2,1)}) %reduce-scatter.2.cloned.1.call-update) | async-done | bytes 1048592 | tf_op jit(solution)/shard_map/reduce_scatter | solution.py:86
  179.5 4.6 %all-to-all-start.1 = ((bf16[128,8,512]{2,0,1:T(8,128)(2,1)}), bf16[128,8,512]{2,0,1:T(8,128)(2,1)S(1)}, u32[]{:S(2)}, u32[]{:S(2)}) async-start(bf16[128,8,512]{2,0,1:T(8,128)(2,1)} %reduce-scatter.2.cloned.1.call-done), calls=%async_computation.2 | async-start | bytes 2097152 | tf_op jit(solution)/shard_map/all_to_all | solution.py:89
  184.1 0.2 fusion.37
  184.3 0.2 fusion.39
  184.5 0.2 fusion.41
  184.8 0.1 multiply_reduce_fusion.2
  184.8 31.5 %all-gather.3.cloned.1.call-done = bf16[512,2048]{1,0:T(8,128)(2,1)} async-done(((bf16[512,512]{1,0:T(8,128)(2,1)}), bf16[512,2048]{1,0:T(8,128)(2,1)}) %all-gather.3.cloned.1.call-update) | async-done | bytes 2097168 | tf_op jit(solution)/shard_map/all_gather | solution.py:67
  216.4 2.5 %multiply_reduce_fusion = (f32[256]{0:T(256)S(1)}, f32[256,2048]{1,0:T(8,128)S(1)}) fusion(bf16[512,2048]{1,0:T(8,128)(2,1)} %all-gather.3.cloned.1.call-done, f32[256,128]{0,1:T(8,128)S(1)} %fusion.35, f32[256,128]{0,1:T(8,128)S(1)} %fusion.37, f32[256,128]{0,1:T(8,128)S(1)} %fusion.39, f32[256,128]{0,1:T(8,128)S(1)} %fusion.41, f32[512]{0:T(512)S(1)} %copy-done.3, ...), kind=kOutput, calls=%fused_computation.12 | convolution fusion | flops 538705664 | bytes 4722688 | tf_op jit(solution)/shard_map/dot_general | solution.py:65
  218.9 1.2 multiply_convert_fusion.1
  220.2 0.6 copy.24
  220.7 2.0 gather_fusion.1
  222.7 0.3 reshape.212
  223.0 1.4 multiply_reduce_fusion.1
  (30 shorter events, 0.2 us)
Async XLA Ops:
  7.2 100.1 %all-gather.5.cloned.1.call-start = ((), (), s32[]{:S(2)}) async-start(), calls=%async_computation.4 | async-start | bytes 5242880 | tf_op jit(solution)/shard_map/all_gather | solution.py:121
  55.6 123.9 %reduce-scatter.2.cloned.1.call-start = ((), (), s32[]{:S(2)}) async-start(), calls=%async_computation.5 | async-start | bytes 5242880 | tf_op jit(solution)/shard_map/reduce_scatter | solution.py:86
  107.3 7.7 %copy-start.6 = (bf16[1,2048,1024]{2,1,0:T(8,128)(2,1)S(1)}, bf16[1,2048,1024]{2,1,0:T(8,128)(2,1)}, u32[]{:S(2)}) copy-start(bf16[1,2048,1024]{2,1,0:T(8,128)(2,1)} %param.23) | copy-start | bytes 12582916
  107.3 7.7 %copy-start.8 = (bf16[128,8,2048]{2,0,1:T(8,128)(2,1)S(1)}, bf16[128,8,2048]{2,0,1:T(8,128)(2,1)}, u32[]{:S(2)}) copy-start(bf16[128,8,2048]{2,0,1:T(8,128)(2,1)} %all-gather.5.cloned.1.call-done) | copy-start | bytes 12582916
  115.0 5.7 %copy-start.7 = (bf16[1,1024,2048]{2,1,0:T(8,128)(2,1)S(1)}, bf16[1,1024,2048]{2,1,0:T(8,128)(2,1)}, u32[]{:S(2)}) copy-start(bf16[1,1024,2048]{2,1,0:T(8,128)(2,1)} %param.24) | copy-start | bytes 12582916
  126.7 0.9 copy-start
  126.7 4.4 %copy-start.5 = (s32[4]{0:T(128)S(1)}, s32[4]{0:T(128)}, u32[]{:S(2)}) copy-start(s32[4]{0:T(128)} %constant.101.clone) | copy-start | bytes 52
  126.7 4.5 %copy-start.4 = (f32[128,4]{0,1:T(4,128)S(1)}, f32[128,4]{0,1:T(4,128)}, u32[]{:S(2)}) copy-start(f32[128,4]{0,1:T(4,128)} %param.21) | copy-start | bytes 6148
  126.7 89.6 %all-gather.3.cloned.1.call-start = ((), (), s32[]{:S(2)}) async-start(), calls=%async_computation.3 | async-start | bytes 2621440 | tf_op jit(solution)/shard_map/all_gather | solution.py:67
  127.7 4.8 %collective-permute-start = (bf16[15,512]{1,0:T(8,128)(2,1)S(1)}, bf16[15,512]{1,0:T(8,128)(2,1)S(1)}, u32[]{:S(2)}, u32[]{:S(2)}) collective-permute-start(bf16[15,512]{1,0:T(8,128)(2,1)S(1)} %slice.82), channel_id=1, source_target_pairs={{0,1},{1,2},{2,3},{3,4},{4,5},{5,6},{6,7},{7,8},{8,9},{9,10},{10,1... | collective-permute-start | bytes 46088 | tf_op jit(solution)/shard_map/ppermute | solution.py:16
  132.6 1.2 copy-start.1
  132.6 83.8 %copy-start.3 = (f32[512]{0:T(512)S(1)}, f32[512]{0:T(512)}, u32[]{:S(2)}) copy-start(f32[512]{0:T(512)} %param.15) | copy-start | bytes 6148
  133.7 85.2 %copy-start.2 = (f32[2048]{0:T(1024)S(1)}, f32[2048]{0:T(1024)}, u32[]{:S(2)}) copy-start(f32[2048]{0:T(1024)} %param.17) | copy-start | bytes 24580
  179.5 40.7 %all-to-all-start.1 = ((bf16[128,8,512]{2,0,1:T(8,128)(2,1)}), bf16[128,8,512]{2,0,1:T(8,128)(2,1)S(1)}, u32[]{:S(2)}, u32[]{:S(2)}) async-start(bf16[128,8,512]{2,0,1:T(8,128)(2,1)} %reduce-scatter.2.cloned.1.call-done), calls=%async_computation.2 | async-start | bytes 2097152 | tf_op jit(solution)/shard_map/all_to_all | solution.py:89
Sparse Core Ops, SparseCore 0:
  55.7 51.4 all-gather.4
  126.9 52.5 reduce-scatter.1
  181.3 35.0 all-gather.2
where the time goes:
time: 231 us
  waiting for transfers between devices  130 us (56%)
  blocking collectives  32.8 us (14%)
  matrix products  22.7 us (10%)
  local copies, waits for them, and re-layouts  15 us (6%)
  between operations  14 us (6%)
  starting transfers between devices  8.11 us (4%)
  other arithmetic  7.78 us (3%)
    all_gather x1, waiting for transfers between devices, per_device(): lax.all_gather(arrived, 'tp', axis=0, tiled=True)  51.6 us
    reduce_scatter x1, waiting for transfers between devices, send_home(): lax.psum_scatter(partial_sum.astype(jnp.bfloat16), 'tp', scatter_dimensio...  45.5 us
    all_to_all x1, blocking collectives, per_device(): lax.all_to_all(my_share, 'ep', split_axis=1, concat_axis=1, tiled=True)  32.8 us
    all_gather x1, waiting for transfers between devices, pool_branch(): lax.all_gather(out_weight, 'tp', axis=1, tiled=True)  31.5 us
    dot_general x1, matrix products, expert_hidden(): jnp.einsum('sed,df->sef', slot_rows, gate_local, preferred_element_type=j...  7.64 us
    dot_general x1, matrix products, send_home(): jnp.einsum('sef,fd->sed', hidden, down_local, preferred_element_type=jnp....  6.07 us
    gather x1, local copies, waits for them, and re-layouts, per_device(): slot_rows = padded[owner_rows].reshape(capacity, expert_count, model_width)  6.02 us
    dot_general x1, matrix products, expert_hidden(): jnp.einsum('sed,df->sef', slot_rows, up_local, preferred_element_type=jnp...  5.65 us
  transfers between devices with their start and end apart: 5, of which 4 were waited for; matrix products, arithmetic and copies ran while one was open for 3% of the time, Pallas kernels for 0%

commit v1 on v0

--- a/solution.py
+++ b/solution.py
@@ -8,6 +8,13 @@
 norm_eps = 1e-06
 clamp_limit = 7.0
 sigmoid_slope = 1.702
+
+
+def stacked_exchange(x, mesh_axis, split, join):
+    peers = lax.axis_size(mesh_axis)
+    shards = jnp.stack(jnp.split(x, peers, axis=split), axis=0)
+    shards = lax.all_to_all(shards, mesh_axis, split_axis=0, concat_axis=0)
+    return jnp.concatenate(shards, axis=join)
 
 
 def shifted_2(block, axis, distance):
@@ -117,7 +124,7 @@
     down_local = down_weight[0]
     share = capacity // lax.axis_size("tp")
     my_share = lax.dynamic_slice_in_dim(slot_rows, lax.axis_index("tp") * share, share, 0)
-    arrived = lax.all_to_all(my_share, "ep", split_axis=1, concat_axis=1, tiled=True)
+    arrived = stacked_exchange(my_share, "ep", 1, 1)
     hidden = expert_hidden(lax.all_gather(arrived, "tp", axis=0, tiled=True), gate_local, up_local)
     returned = send_home(hidden, down_local)
     column_count = returned.shape[2]

time: 231 us -> 243 us (1.052)
  matrix products: 22.7 us -> 29.2 us
  local copies, waits for them, and re-layouts: 15 us -> 20.8 us
    dot_general x1, matrix products: 6.07 us -> 15.9 us  [send_home(): jnp.einsum('sef,fd->sed', hidden, down_local, preferred_element_type=jnp....]
    split x0 -> x1, local copies, waits for them, and re-layouts: none -> 6.99 us  [stacked_exchange(): shards = jnp.stack(jnp.split(x, peers, axis=split), axis=0)]
    dot_general x1 -> x0, matrix products: 5.65 us -> none  [expert_hidden(): jnp.einsum('sed,df->sef', slot_rows, up_local, preferred_element_type=jnp...]
where the time goes in v1:
time: 243 us
  waiting for transfers between devices  130 us (53%)
  blocking collectives  32.8 us (13%)
  matrix products  29.2 us (12%)
  local copies, waits for them, and re-layouts  20.8 us (9%)
  between operations  14 us (6%)
  starting transfers between devices  8.26 us (3%)
  other arithmetic  7.78 us (3%)
    all_gather x1, waiting for transfers between devices, per_device(): lax.all_gather(arrived, 'tp', axis=0, tiled=True)  51.3 us
    reduce_scatter x1, waiting for transfers between devices, send_home(): lax.psum_scatter(partial_sum.astype(jnp.bfloat16), 'tp', scatter_dimensio...  45.6 us
    all_to_all x1, blocking collectives, stacked_exchange(): shards = lax.all_to_all(shards, mesh_axis, split_axis=0, concat_axis=0)  32.8 us
    all_gather x1, waiting for transfers between devices, pool_branch(): lax.all_gather(out_weight, 'tp', axis=1, tiled=True)  31.6 us
    dot_general x1, matrix products, send_home(): jnp.einsum('sef,fd->sed', hidden, down_local, preferred_element_type=jnp....  15.9 us
    dot_general x1, matrix products, expert_hidden(): jnp.einsum('sed,df->sef', slot_rows, gate_local, preferred_element_type=j...  9.93 us
    split x1, local copies, waits for them, and re-layouts, stacked_exchange(): shards = jnp.stack(jnp.split(x, peers, axis=split), axis=0)  6.99 us
    gather x1, local copies, waits for them, and re-layouts, per_device(): slot_rows = padded[owner_rows].reshape(capacity, expert_count, model_width)  6.02 us
  transfers between devices with their start and end apart: 5, of which 4 were waited for; matrix products, arithmetic and copies ran while one was open for 3% of the time, Pallas kernels for 0%

profile of v1, /device:TPU:0, one launch (start us, length us, event | category | flops | bytes accessed | tf_op | source)
XLA Modules:
  0.0 243.0 jit_solution(16158029660392935601)
XLA Ops:
  7.2 0.8 copy.112
  8.0 0.1 eq.29
  8.1 0.1 eq.25
  8.2 0.1 reshape.215
  8.4 1.1 reduce-window.6
  9.5 0.2 slice_reduce_fusion
  9.8 0.1 fusion.64
  9.9 2.4 %scatter_custom_fusion = s32[1024]{0:T(1024)S(1)} fusion(s32[512]{0:T(512)S(1)} %bitcast.94, s32[512]{0:T(512)S(1)} %add_select_fusion, s32[]{:T(128)} %constant.34.clone.1), kind=kCustom, calls=%fused_computation.123 | custom fusion | bytes 4100 | tf_op jit(solution)/shard_map/scatter | solution.py:40
  12.3 1.2 fusion.23
  13.6 1.2 fusion.25
  14.9 6.0 %gather_fusion = bf16[1024,2048]{1,0:T(8,128)(2,1)} fusion(bf16[129,2048]{1,0:T(8,128)(2,1)S(1)} %concatenate.11, s32[1024]{0:T(1024)S(1)} %fusion.66), kind=kCustom, calls=%fused_computation | custom fusion | bytes 8392704 | tf_op jit(solution)/shard_map/gather | solution.py:121
  20.9 7.0 %constant_dynamic-slice_fusion.7 = (bf16[32,1,2048]{2,1,0:T(2,128)(2,1)S(1)}, bf16[32,1,2048]{2,1,0:T(2,128)(2,1)S(1)}, bf16[32,1,2048]{2,1,0:T(2,128)(2,1)S(1)}...) fusion(bf16[128,8,2048]{2,1,0:T(8,128)(2,1)} %bitcast.92, ...), kind=kLoop, calls=%fused_computation.132 | loop fusion | bytes 2097184 | tf_op jit(solution)/shard_map/split | solution.py:15
  27.9 0.1 bitcast_dynamic-update-slice_fusion.7
  28.0 0.1 bitcast_dynamic-update-slice_fusion.6
  28.1 0.1 bitcast_dynamic-update-slice_fusion.5
  28.2 0.1 bitcast_dynamic-update-slice_fusion.4
  28.3 0.1 bitcast_dynamic-update-slice_fusion.3
  28.3 0.1 bitcast_dynamic-update-slice_fusion.2
  28.4 0.1 bitcast_dynamic-update-slice_fusion.1
  28.5 0.1 bitcast_dynamic-update-slice_fusion
  28.6 32.8 %all_to_all.10 = bf16[8,32,1,2048]{3,1,2,0:T(8,128)(2,1)} all-to-all(bf16[8,32,1,2048]{3,1,2,0:T(8,128)(2,1)S(1)} %bitcast_dynamic-update-slice_fusion), channel_id=1, replica_groups=mesh['ep'=8,'tp'=4] {'ep'}, dimensions={0} | all-to-all | bytes 2097152 | tf_op jit(solution)/shard_map/all_to_all | solution.py:16
  61.5 0.2 reduce-scatter.2.cloned.1.call-start
  61.7 51.3 %all-gather.6.cloned.1.call-done = bf16[128,8,1,2048]{3,0,1,2:T(8,128)(2,1)} async-done(((bf16[32,8,1,2048]{3,0,1,2:T(8,128)(2,1)}), bf16[128,8,1,2048]{3,0,1,2:T(8,128)(2,1)}) %all-gather.6.cloned.1.call-update) | async-done | bytes 4194320 | tf_op jit(solution)/shard_map/all_gather | solution.py:128
  113.0 9.9 %fusion.2 = f32[128,8,1024]{2,0,1:T(8,128)} fusion(bf16[1,2048,1024]{2,1,0:T(8,128)(2,1)} %param.22, bf16[128,8,1,2048]{3,0,1,2:T(8,128)(2,1)} %all-gather.6.cloned.1.call-done), kind=kOutput, calls=%fused_computation.5 | convolution fusion | flops 4294967296 | bytes 12582912 | tf_op jit(solution)/shard_map/sed,df->sef/dot_general | solution.py:81
  122.9 15.9 %fusion.8 = bf16[128,8,2048]{2,0,1:T(8,128)(2,1)} fusion(bf16[1,1024,2048]{2,1,0:T(8,128)(2,1)} %param.24, f32[128,8,1024]{2,0,1:T(8,128)} %fusion.2, bf16[1,2048,1024]{2,1,0:T(8,128)(2,1)} %param.23, bf16[128,8,1,2048]{3,0,1,2:T(8,128)(2,1)} %all-gather.6.cloned.1.call-done), kind=kOutput, calls=%fused_computation.12 | convolution fusion | flops 8602517504 | bytes 20971520 | tf_op jit(solution)/shard_map/sef,fd->sed/dot_general | solution.py:91
  138.9 0.7 all-gather.4.cloned.1.call-update
  139.5 0.2 copy-done
  139.7 3.4 %collective-permute-start = (bf16[15,512]{1,0:T(8,128)(2,1)S(1)}, bf16[15,512]{1,0:T(8,128)(2,1)S(1)}, u32[]{:S(2)}, u32[]{:S(2)}) collective-permute-start(bf16[15,512]{1,0:T(8,128)(2,1)S(1)} %slice.82), channel_id=1, source_target_pairs={{0,1},{1,2},{2,3},{3,4},{4,5},{5,6},{6,7},{7,8},{8,9},{9,10},{10,1... | collective-permute-start | bytes 46088 | tf_op jit(solution)/shard_map/ppermute | solution.py:23
  143.1 0.1 broadcast_bitcast_fusion
  143.2 0.1 bitcast_compare_fusion.15
  143.3 0.1 copy.117
  143.4 1.1 collective-permute-done
  144.5 0.1 maximum_convert_fusion
  144.6 1.1 fusion.43
  145.8 0.2 fusion.47
  146.0 45.6 %reduce-scatter.2.cloned.1.call-done = bf16[128,8,512]{2,0,1:T(8,128)(2,1)} async-done(((bf16[128,8,2048]{2,0,1:T(8,128)(2,1)}), bf16[128,8,512]{2,0,1:T(8,128)(2,1)}) %reduce-scatter.2.cloned.1.call-update) | async-done | bytes 1048592 | tf_op jit(solution)/shard_map/reduce_scatter | solution.py:93
  191.6 4.6 %all-to-all-start.1 = ((bf16[128,8,512]{2,0,1:T(8,128)(2,1)}), bf16[128,8,512]{2,0,1:T(8,128)(2,1)S(1)}, u32[]{:S(2)}, u32[]{:S(2)}) async-start(bf16[128,8,512]{2,0,1:T(8,128)(2,1)} %reduce-scatter.2.cloned.1.call-done), calls=%async_computation.2 | async-start | bytes 2097152 | tf_op jit(solution)/shard_map/all_to_all | solution.py:96
  196.2 0.2 fusion.49
  196.4 0.2 fusion.51
  196.6 0.2 fusion.53
  196.8 0.1 multiply_reduce_fusion.2
  196.9 31.6 %all-gather.4.cloned.1.call-done = bf16[512,2048]{1,0:T(8,128)(2,1)} async-done(((bf16[512,512]{1,0:T(8,128)(2,1)}), bf16[512,2048]{1,0:T(8,128)(2,1)}) %all-gather.4.cloned.1.call-update) | async-done | bytes 2097168 | tf_op jit(solution)/shard_map/all_gather | solution.py:74
  228.5 2.5 %multiply_reduce_fusion = (f32[256]{0:T(256)S(1)}, f32[256,2048]{1,0:T(8,128)S(1)}) fusion(bf16[512,2048]{1,0:T(8,128)(2,1)} %all-gather.4.cloned.1.call-done, f32[256,128]{0,1:T(8,128)S(1)} %fusion.47, f32[256,128]{0,1:T(8,128)S(1)} %fusion.49, f32[256,128]{0,1:T(8,128)S(1)} %fusion.51, f32[256,128]{0,1:T(8,128)S(1)} %fusion.53, f32[512]{0:T(512)S(1)} %copy-done.3, ...), kind=kOutput, calls=%fused_computation.18 | convolution fusion | flops 538705664 | bytes 4722688 | tf_op jit(solution)/shard_map/dot_general | solution.py:72
  231.0 1.2 multiply_convert_fusion.1
  232.2 0.6 copy.135
  232.8 2.0 gather_fusion.1
  234.8 0.3 reshape.220
  235.1 1.4 multiply_reduce_fusion.1
  (30 shorter events, 0.3 us)
Async XLA Ops:
  7.2 105.8 %all-gather.6.cloned.1.call-start = ((), (), s32[]{:S(2)}) async-start(), calls=%async_computation.5 | async-start | bytes 5242880 | tf_op jit(solution)/shard_map/all_gather | solution.py:128
  61.5 130.1 %reduce-scatter.2.cloned.1.call-start = ((), (), s32[]{:S(2)}) async-start(), calls=%async_computation.4 | async-start | bytes 5242880 | tf_op jit(solution)/shard_map/reduce_scatter | solution.py:93
  138.8 0.9 copy-start
  138.8 4.3 %copy-start.5 = (s32[4]{0:T(128)S(1)}, s32[4]{0:T(128)}, u32[]{:S(2)}) copy-start(s32[4]{0:T(128)} %constant.101.clone) | copy-start | bytes 52
  138.8 4.5 %copy-start.4 = (f32[128,4]{0,1:T(4,128)S(1)}, f32[128,4]{0,1:T(4,128)}, u32[]{:S(2)}) copy-start(f32[128,4]{0,1:T(4,128)} %param.21) | copy-start | bytes 6148
  138.8 89.7 %all-gather.4.cloned.1.call-start = ((), (), s32[]{:S(2)}) async-start(), calls=%async_computation.3 | async-start | bytes 2621440 | tf_op jit(solution)/shard_map/all_gather | solution.py:74
  139.7 4.8 %collective-permute-start = (bf16[15,512]{1,0:T(8,128)(2,1)S(1)}, bf16[15,512]{1,0:T(8,128)(2,1)S(1)}, u32[]{:S(2)}, u32[]{:S(2)}) collective-permute-start(bf16[15,512]{1,0:T(8,128)(2,1)S(1)} %slice.82), channel_id=1, source_target_pairs={{0,1},{1,2},{2,3},{3,4},{4,5},{5,6},{6,7},{7,8},{8,9},{9,10},{10,1... | collective-permute-start | bytes 46088 | tf_op jit(solution)/shard_map/ppermute | solution.py:23
  144.6 1.2 copy-start.1
  144.6 83.9 %copy-start.3 = (f32[512]{0:T(512)S(1)}, f32[512]{0:T(512)}, u32[]{:S(2)}) copy-start(f32[512]{0:T(512)} %param.15) | copy-start | bytes 6148
  145.8 85.2 %copy-start.2 = (f32[2048]{0:T(1024)S(1)}, f32[2048]{0:T(1024)}, u32[]{:S(2)}) copy-start(f32[2048]{0:T(1024)} %param.17) | copy-start | bytes 24580
  191.6 40.7 %all-to-all-start.1 = ((bf16[128,8,512]{2,0,1:T(8,128)(2,1)}), bf16[128,8,512]{2,0,1:T(8,128)(2,1)S(1)}, u32[]{:S(2)}, u32[]{:S(2)}) async-start(bf16[128,8,512]{2,0,1:T(8,128)(2,1)} %reduce-scatter.2.cloned.1.call-done), calls=%async_computation.2 | async-start | bytes 2097152 | tf_op jit(solution)/shard_map/all_to_all | solution.py:96
Sparse Core Ops, SparseCore 0:
  61.6 51.3 all-gather.5
  138.9 52.5 reduce-scatter.1
  193.4 35.0 all-gather.3
